TPU v7x, 32 devices: a whole 2x2x4 slice. The times are simulated.
32 devices in a mesh: fs: 16 (over z, y, x), tp: 2 (over core).
Axes of the slice: x: 2, y: 2, z: 4, core: 2. Of those that a mesh axis runs over, the one named last changes fastest.
Arguments:
- tokens: bfloat16 [12288, 2048], P('fs'), may hold values from -6 to 6
- norm_gain: float32 [2048], replicated, may hold values from 0.1 to 1.9
- up_weight: float32 [2048, 8192], P('fs', 'tp'), may hold values from -0.125 to 0.125
- up_scale: float32 [8192], P('tp'), may hold values from 0.5 to 2
- down_weight: float32 [8192, 2048], P('tp', 'fs'), may hold values from -0.0625 to 0.0625
- down_scale: float32 [2048], P('fs'), may hold values from 0.5 to 2
Outputs:
- output: bfloat16 [12288, 2048], P('fs', 'tp')
All inputs are finite; a program needn't handle non-finite values.
Results may differ from a plain program's by a relative error of at most 0.015.
Values may be sent and summed in bfloat16 or wider, within the bound.
A program may use at most 128 MiB of HBM per device.

v0:
```python
import jax
import jax.numpy as jnp
from jax import lax
from jax.sharding import PartitionSpec as P

epsilon = 1e-06


def local(tokens, norm_gain, up_weight, up_scale, down_weight, down_scale):
    floats = tokens.astype(jnp.float32)
    inverse = lax.rsqrt(jnp.mean(floats * floats, axis=-1, keepdims=True) + epsilon)
    normed = (floats * inverse * norm_gain).astype(jnp.bfloat16)
    up_half = up_weight.astype(jnp.bfloat16)
    down_half = down_weight.astype(jnp.bfloat16)
    up_pre = jnp.dot(
        normed,
        lax.all_gather(up_half, "fs", axis=0, tiled=True),
        preferred_element_type=jnp.float32,
    )
    down_whole, scale_whole = (
        lax.all_gather(down_half, "fs", axis=1, tiled=True),
        lax.all_gather(down_scale.astype(jnp.bfloat16), "fs", axis=0, tiled=True).astype(
            down_scale.dtype
        ),
    )
    hidden = jnp.square(jax.nn.relu(up_pre * up_scale)).astype(jnp.bfloat16)
    partial_value = jnp.dot(hidden, down_whole, preferred_element_type=jnp.float32).astype(
        jnp.bfloat16
    )
    summed = lax.psum_scatter(
        partial_value.astype(jnp.float32).astype(jnp.bfloat16),
        "tp",
        scatter_dimension=1,
        tiled=True,
    ).astype(jnp.float32)
    own_width = summed.shape[1]
    own_scale = lax.dynamic_slice_in_dim(
        scale_whole, lax.axis_index("tp") * own_width, own_width, 0
    )
    return (summed * own_scale).astype(jnp.bfloat16)


def solution(mesh):
    in_specs = (P("fs", None), P(), P("fs", "tp"), P("tp"), P("tp", "fs"), P("fs"))
    out_specs = P("fs", "tp")
    return jax.shard_map(local, mesh=mesh, in_specs=in_specs, out_specs=out_specs, check_vma=False)
```

profile of v0, /device:TPU:0, one launch (start us, length us, event | category | flops | bytes accessed | tf_op | source)
XLA Modules:
  0.0 539.5 jit_solution(17070823121638339327)
XLA Ops:
  6.5 0.0 copy-start
  6.5 0.0 copy-start.1
  6.5 0.0 copy-start.2
  6.5 0.0 all-gather.6.cloned.1.call-start
  6.5 2.8 convert_element_type.36
  9.4 0.0 all-gather.6.cloned.1.call-update
  9.4 0.0 all-gather.4.cloned.1.call-start
  9.4 2.7 convert_element_type.34
  12.1 0.0 all-gather.4.cloned.1.call-update
  12.2 0.0 reduce-scatter.2.cloned.1.call-start
  12.2 0.0 copy-done
  12.2 0.7 fusion
  12.9 0.0 copy-start.3
  12.9 249.0 %all-gather.6.cloned.1.call-done = bf16[4096,2048]{1,0:T(8,128)(2,1)} async-done(((bf16[4096,128]{1,0:T(8,128)(2,1)}), bf16[4096,2048]{1,0:T(8,128)(2,1)}) %all-gather.6.cloned.1.call-update) | async-done | bytes 16777232 | tf_op jit(solution)/shard_map/all_gather | solution.py:21
  261.9 192.0 %all-gather.4.cloned.1.call-done = bf16[2048,4096]{1,0:T(8,128)(2,1)} async-done(((bf16[128,4096]{1,0:T(8,128)(2,1)}), bf16[2048,4096]{1,0:T(8,128)(2,1)}) %all-gather.4.cloned.1.call-update) | async-done | bytes 16777232 | tf_op jit(solution)/shard_map/all_gather | solution.py:17
  453.9 0.0 copy-done.1
  453.9 0.0 copy-done.2
  453.9 38.2 %convolution_convert_fusion = bf16[768,2048]{1,0:T(8,128)(2,1)} fusion(bf16[4096,2048]{1,0:T(8,128)(2,1)} %all-gather.6.cloned.1.call-done, bf16[2048,4096]{1,0:T(8,128)(2,1)} %all-gather.4.cloned.1.call-done, f32[4096]{0:T(1024)S(1)} %copy-done.1, bf16[768,2048]{1,0:T(8,128)(2,1)S(1)} %copy-done, f32[2048]{0:T(1024)S(1)} %copy-done.2, ...), kind=kOutput, calls=%fused_computation.6 | convolution fusion | flops 25790251008 | bytes 39873536 | tf_op jit(solution)/shard_map/dot_general | solution.py:27
  492.1 0.0 reduce-scatter.2.cloned.1.call-update
  492.2 0.0 copy-done.3
  492.2 37.8 %all-gather = bf16[16,1,128]{2,1,0:T(2,128)(2,1)S(1)} all-gather(bf16[1,1,128]{2,1,0:T(2,128)(2,1)S(1)} %convert_bitcast_fusion), channel_id=1, replica_groups=mesh['fs'=16,'tp'=2] {'fs'}, dimensions={0}, use_global_device_ids=true | all-gather | bytes 4352 | tf_op jit(solution)/shard_map/all_gather | solution.py:22
  530.0 0.0 reduce-scatter.2.cloned.1.call-done
  530.0 3.0 multiply_convert_fusion.1
  (4 shorter events, 0.0 us)
Async XLA Ops:
  6.5 5.7 %copy-start = (bf16[768,2048]{1,0:T(8,128)(2,1)S(1)}, bf16[768,2048]{1,0:T(8,128)(2,1)}, u32[]{:S(2)}) copy-start(bf16[768,2048]{1,0:T(8,128)(2,1)} %param.6) | copy-start | bytes 9437188
  6.5 447.4 %copy-start.1 = (f32[4096]{0:T(1024)S(1)}, f32[4096]{0:T(1024)}, u32[]{:S(2)}) copy-start(f32[4096]{0:T(1024)} %param.9) | copy-start | bytes 49156
  6.5 447.4 %copy-start.2 = (f32[2048]{0:T(1024)S(1)}, f32[2048]{0:T(1024)}, u32[]{:S(2)}) copy-start(f32[2048]{0:T(1024)} %param.7) | copy-start | bytes 24580
  6.5 255.4 %all-gather.6.cloned.1.call-start = ((), (), s32[]{:S(2)}) async-start(), calls=%async_computation.2 | async-start | bytes 17825792 | tf_op jit(solution)/shard_map/all_gather | solution.py:21
  9.4 444.5 %all-gather.4.cloned.1.call-start = ((), (), s32[]{:S(2)}) async-start(), calls=%async_computation.1 | async-start | bytes 17825792 | tf_op jit(solution)/shard_map/all_gather | solution.py:17
  12.2 517.9 %reduce-scatter.2.cloned.1.call-start = ((), (), s32[]{:S(2)}) async-start(), calls=%async_computation.3 | async-start | bytes 4718592 | tf_op jit(solution)/shard_map/reduce_scatter | solution.py:30
  12.9 479.3 %copy-start.3 = (f32[128]{0:T(128)S(1)}, f32[128]{0:T(128)}, u32[]{:S(2)}) copy-start(f32[128]{0:T(128)} %param.11) | copy-start | bytes 1540
Sparse Core Ops, SparseCore 0:
  10.0 251.8 all-gather.5
  264.7 189.1 all-gather.3
  492.3 9.1 reduce-scatter.1
where the time goes:
time: 540 us
  waiting for transfers between devices  441 us (82%)
  matrix products  38.2 us (7%)
  blocking collectives  37.8 us (7%)
  between operations  13.2 us (2%)
  other arithmetic  9.18 us (2%)
    all_gather x1, waiting for transfers between devices, local(): lax.all_gather(down_half, 'fs', axis=1, tiled=True)  249 us
    all_gather x1, waiting for transfers between devices, local(): lax.all_gather(up_half, 'fs', axis=0, tiled=True)  192 us
    dot_general x1, matrix products, local(): jnp.dot(hidden, down_whole, preferred_element_type=jnp.float32)  38.2 us
    all_gather x1, blocking collectives, local(): lax.all_gather(down_scale.astype(jnp.bfloat16), 'fs', axis=0, tiled=True)  37.8 us
  transfers between devices with their start and end apart: 3, of which 2 were waited for; matrix products, arithmetic and copies ran while one was open for 1% of the time, Pallas kernels for 0%

commit v1 on v0

v1 whole, which is shorter than its diff:
```python
import functools

import jax
import jax.numpy as jnp
from jax import lax
from jax.experimental import pallas as pl
from jax.experimental.pallas import tpu as pltpu
from jax.sharding import PartitionSpec as P

epsilon = 1e-06


def normalise(tokens, norm_gain):
    floats = tokens.astype(jnp.float32)
    inverse = lax.rsqrt(jnp.mean(floats * floats, axis=-1, keepdims=True) + epsilon)
    return (floats * inverse * norm_gain).astype(jnp.bfloat16)


def plain(tokens, norm_gain, up_weight, up_scale, down_weight, down_scale):
    normed = normalise(tokens, norm_gain)
    up_whole = lax.all_gather(up_weight.astype(jnp.bfloat16), "fs", axis=0, tiled=True)
    up_pre = jnp.dot(normed, up_whole, preferred_element_type=jnp.float32)
    scaled = (down_weight * down_scale).astype(jnp.bfloat16)
    down_whole = lax.all_gather(scaled, "fs", axis=1, tiled=True)
    hidden = jnp.square(jax.nn.relu(up_pre * up_scale)).astype(jnp.bfloat16)
    partial_value = jnp.dot(hidden, down_whole, preferred_element_type=jnp.float32)
    return lax.psum_scatter(
        partial_value.astype(jnp.bfloat16), "tp", scatter_dimension=1, tiled=True
    )


NX, NY = 2, 2


def kernel(nz, x_ref, s_ref, up_ref, down_ref, out_ref,
           u_buf, d_buf, t_buf, h_buf, ssend, srecv, xsend, xrecv, keep,
           send_sems, recv_sems, local_sems):
    me = lax.axis_index("fs")
    c = lax.axis_index("tp")
    x = lax.rem(me, NX)
    y = lax.rem(me // NX, NY)
    z = me // (NX * NY)
    rows = x_ref.shape[0]
    depth = up_ref.shape[0]
    wide = up_ref.shape[1] // NX
    cols = down_ref.shape[1]
    pair = NX * cols

    def fs_of(zz, yy, xx):
        return (zz * NY + yy) * NX + xx

    def wrap(v):
        return lax.rem(v + 2 * nz, nz)

    target = {
        "z+": {"fs": fs_of(wrap(z + 1), y, x), "tp": c},
        "z-": {"fs": fs_of(wrap(z - 1), y, x), "tp": c},
        "y": {"fs": fs_of(z, 1 - y, x), "tp": c},
        "x": {"fs": fs_of(z, y, 1 - x), "tp": c},
        "c": {"fs": me, "tp": 1 - c},
    }

    local = [
        pltpu.make_async_copy(
            up_ref.at[:, pl.ds(pl.multiple_of(x * wide, wide), wide)],
            u_buf.at[pl.ds(pl.multiple_of(me * depth, depth), depth), :], local_sems.at[0]),
        pltpu.make_async_copy(
            down_ref.at[pl.ds(pl.multiple_of(x * wide, wide), wide), :],
            d_buf.at[me // NX, :, pl.ds(pl.multiple_of(x * cols, cols), cols)], local_sems.at[1]),
    ]
    for copy in local:
        copy.start()

    barrier = pltpu.get_barrier_semaphore()
    for where in target.values():
        pl.semaphore_signal(barrier, inc=1, device_id=where, device_id_type=pl.DeviceIdType.MESH)
    pl.semaphore_wait(barrier, len(target))

    slots, started = {}, []

    def copy_of(key, src, dst, way):
        n = slots.setdefault(key, len(slots))
        return pltpu.make_async_remote_copy(
            src_ref=src, dst_ref=dst, send_sem=send_sems.at[n], recv_sem=recv_sems.at[n],
            device_id=target[way], device_id_type=pl.DeviceIdType.MESH)

    def launch(key, src, dst, way):
        copy = copy_of(key, src, dst, way)
        copy.start()
        started.append(copy)

    def arrive(key, dst, way="x"):
        copy_of(key, dst, dst, way).wait_recv()

    def block(kind, part, dz, dy, half):
        zz, yy = wrap(z + dz), lax.rem(y + dy, NY)
        xx = x if part == "A" else 1 - x
        if kind == "U":
            size = depth if half is None else depth // 2
            at = fs_of(zz, yy, xx) * depth + (0 if half in (None, 0) else size)
            return u_buf.at[pl.ds(pl.multiple_of(at, size), size), :]
        size = wide if half is None else wide // 2
        at = 0 if half in (None, 0) else size
        return d_buf.at[zz * NY + yy, pl.ds(at, size), pl.ds(pl.multiple_of(xx * cols, cols), cols)]

    def send(kind, part, dz, dy, way, half=None):
        ref = block(kind, part, dz, dy, half)
        to = {"z+": ((dz - 1) % nz, dy), "z-": ((dz + 1) % nz, dy), "y": (dz % nz, 1 - dy)}[way]
        launch((kind, part) + to + (half,), ref, ref, way)

    def take(kind, part, dz, dy, half=None):
        arrive((kind, part, dz % nz, dy, half), block(kind, part, dz, dy, half))

    def g1(k):
        for way in ("z+", "z-", "y"):
            send(k, "A", 0, 0, way)

    def g2(k):
        take(k, "B", 0, 0)
        for way in ("y", "z+", "z-"):
            send(k, "B", 0, 0, way)

    def g3(k):
        for dz, way, half in ((-1, "z+", 0), (1, "z-", 1)):
            take(k, "A", dz, 0)
            send(k, "A", dz, 0, way, half)
            send(k, "A", dz, 0, "y")

    def g4(k):
        take(k, "B", 0, 1)
        for way in ("z+", "z-"):
            send(k, "B", 0, 1, way)

    def g5(k):
        for dz, way, half in ((-1, "z+", 0), (1, "z-", 1)):
            take(k, "B", dz, 0)
            send(k, "B", dz, 0, way, half)

    def g6(k):
        take(k, "A", 2, 0, 0)
        take(k, "A", 2, 0, 1)
        send(k, "A", 2, 0, "y")

    def g7(k):
        for dz, way, half in ((-1, "z+", 0), (1, "z-", 1)):
            take(k, "B", dz, 1)
            send(k, "B", dz, 1, way, half)

    launch(("U", "B", 0, 0, None),
           up_ref.at[:, pl.ds(pl.multiple_of((1 - x) * wide, wide), wide)],
           u_buf.at[pl.ds(pl.multiple_of(me * depth, depth), depth), :], "x")
    part_rows = rows // 2
    mine_rows = pl.ds(pl.multiple_of(c * part_rows, part_rows), part_rows)
    other_rows = pl.ds(pl.multiple_of((1 - c) * part_rows, part_rows), part_rows)
    launch(("T", "x"), x_ref.at[mine_rows, :], t_buf.at[mine_rows, :], "x")
    launch(("D", "B", 0, 0, None),
           down_ref.at[pl.ds(pl.multiple_of((1 - x) * wide, wide), wide), :],
           d_buf.at[me // NX, :, pl.ds(pl.multiple_of(x * cols, cols), cols)], "x")

    local[0].wait()
    g1("U")
    g2("U")
    g3("U")
    g4("U")
    g5("U")
    g6("U")
    g7("U")
    local[1].wait()
    g1("D")
    arrive(("T", "x"), t_buf.at[mine_rows, :])
    launch(("T", "c"), t_buf.at[mine_rows, :], t_buf.at[mine_rows, :], "c")
    take("U", "A", 0, 1)
    take("U", "A", -1, 1)
    take("U", "A", 1, 1)
    for half in (0, 1):
        take("U", "B", 2, 0, half)
        take("U", "B", 2, 1, half)
    take("U", "A", 2, 1)
    arrive(("T", "c"), t_buf.at[other_rows, :])

    tile_m, tile_n = 256, min(512, wide)

    def up_part(src, base):
        @pl.loop(0, wide // tile_n)
        def _(j):
            at = pl.ds(pl.multiple_of(j * tile_n, tile_n), tile_n)

            @pl.loop(0, rows // tile_m)
            def _(i):
                r = pl.multiple_of(i * tile_m, tile_m)
                pre = jnp.dot(src[pl.ds(r, tile_m), :], u_buf[:, at],
                              preferred_element_type=jnp.float32)
                act = jnp.square(jnp.maximum(pre * s_ref[:, at], 0.0))
                h_buf[pl.ds(base + r, tile_m), at] = act.astype(jnp.bfloat16)

    up_part(x_ref, 0)
    g2("D")
    g3("D")
    up_part(t_buf, rows)
    g4("D")
    g5("D")
    g6("D")
    g7("D")

    stages = [((z + 1) % 2, 0), ((z + 1) % 2, 1), (z % 2, 0), (z % 2, 1)]

    def owned(n, core):
        q, dy = stages[n]
        return (q + core * (nz // 2)) * NY + lax.rem(y + dy, NY)

    def theirs(n):
        zy = owned(n, 1 - c)

        @pl.loop(0, NX * rows // tile_m)
        def _(i):
            r = pl.ds(pl.multiple_of(i * tile_m, tile_m), tile_m)
            ssend[n, r, :] = jnp.dot(h_buf[r, :], d_buf[zy],
                                     preferred_element_type=jnp.float32).astype(jnp.bfloat16)

        launch(("S", n), ssend.at[n], srecv.at[n], "c")

    def mine(n):
        zy = owned(n, c)
        arrive(("S", n), srecv.at[n])

        def total(i):
            r = pl.ds(pl.multiple_of(i, tile_m), tile_m)
            return jnp.dot(h_buf[r, :], d_buf[zy],
                           preferred_element_type=jnp.float32) + srecv[n, r, :].astype(jnp.float32)

        @pl.loop(0, rows // tile_m)
        def _(i):
            r = pl.multiple_of(i * tile_m, tile_m)
            xsend[n, pl.ds(r, tile_m), :] = total(rows + r).astype(jnp.bfloat16)

        launch(("X", n), xsend.at[n], xrecv.at[n], "x")

        @pl.loop(0, rows // tile_m)
        def _(i):
            r = pl.multiple_of(i * tile_m, tile_m)
            keep[n, pl.ds(r, tile_m), :] = total(r)

    def finish(n):
        arrive(("X", n), xrecv.at[n])
        at = pl.multiple_of((owned(n, c) - c * (nz // 2) * NY) * pair, pair)
        out_ref[:, pl.ds(at, pair)] = (keep[n] + xrecv[n].astype(jnp.float32)).astype(out_ref.dtype)

    theirs(0)
    take("D", "A", 0, 1)
    take("D", "A", -1, 1)
    take("D", "A", 1, 1)
    theirs(1)
    mine(0)
    take("D", "B", 2, 0, 0)
    take("D", "B", 2, 0, 1)
    theirs(2)
    mine(1)
    finish(0)
    take("D", "A", 2, 1)
    take("D", "B", 2, 1, 0)
    take("D", "B", 2, 1, 1)
    theirs(3)
    mine(2)
    mine(3)
    finish(1)
    finish(2)
    finish(3)
    for copy in started:
        copy.wait_send()


def fused(nz, tokens, norm_gain, up_weight, up_scale, down_weight, down_scale):
    rows, width = tokens.shape
    depth, hidden = up_weight.shape
    cols = down_weight.shape[1]
    wide = hidden // NX
    x = lax.rem(lax.axis_index("fs"), NX)
    own_scale = lax.dynamic_slice_in_dim(up_scale, x * wide, wide, 0)[None]
    ways = 2 * (8 + 10) + 2 + 8
    vmem = pl.BlockSpec(memory_space=pltpu.VMEM)
    return pl.pallas_call(
        functools.partial(kernel, nz),
        out_shape=jax.ShapeDtypeStruct((rows, width // 2), jnp.bfloat16),
        in_specs=[vmem] * 4,
        out_specs=vmem,
        scratch_shapes=[
            pltpu.VMEM((width, wide), jnp.bfloat16),
            pltpu.VMEM((nz * NY, wide, NX * cols), jnp.bfloat16),
            pltpu.VMEM((rows, width), jnp.bfloat16),
            pltpu.VMEM((NX * rows, wide), jnp.bfloat16),
            pltpu.VMEM((4, NX * rows, NX * cols), jnp.bfloat16),
            pltpu.VMEM((4, NX * rows, NX * cols), jnp.bfloat16),
            pltpu.VMEM((4, rows, NX * cols), jnp.bfloat16),
            pltpu.VMEM((4, rows, NX * cols), jnp.bfloat16),
            pltpu.VMEM((4, rows, NX * cols), jnp.float32),
            pltpu.SemaphoreType.DMA((ways,)),
            pltpu.SemaphoreType.DMA((ways,)),
            pltpu.SemaphoreType.DMA((2,)),
        ],
        compiler_params=pltpu.CompilerParams(
            collective_id=0, has_side_effects=True, vmem_limit_bytes=60 * 1024 * 1024
        ),
    )(
        normalise(tokens, norm_gain),
        own_scale,
        up_weight.astype(jnp.bfloat16),
        (down_weight * down_scale).astype(jnp.bfloat16),
    )


def solution(mesh):
    in_specs = (P("fs", None), P(), P("fs", "tp"), P("tp", "fs"), P("fs"))
    in_specs = in_specs[:3] + (P("tp"),) + in_specs[3:]
    out_specs = P("fs", "tp")
    nz = mesh.shape["fs"] // (NX * NY)
    local = functools.partial(fused, nz) if nz == 4 and mesh.shape["tp"] == 2 else plain
    return jax.shard_map(local, mesh=mesh, in_specs=in_specs, out_specs=out_specs, check_vma=False)
```

time: 540 us -> 245 us (0.45)
  waiting for transfers between devices: 441 us -> 0 us
  Pallas kernels: 0 us -> 234 us
  matrix products: 38.2 us -> 0 us
  blocking collectives: 37.8 us -> 0 us
  between operations: 13.2 us -> 0.03 us
    all_gather x2 -> x0, waiting for transfers between devices: 441 us -> none  [the longest x1 249 us: local(): lax.all_gather(down_half, 'fs', axis=1, tiled=True)]
    pallas_call x0 -> x1, Pallas kernels: none -> 234 us  [fused(): pl.pallas_call(functools.partial(kernel, nz), out_shape=jax.ShapeDtypeStr...]
    dot_general x1 -> x0, matrix products: 38.2 us -> none  [local(): jnp.dot(hidden, down_whole, preferred_element_type=jnp.float32)]
    all_gather x1 -> x0, blocking collectives: 37.8 us -> none  [local(): lax.all_gather(down_scale.astype(jnp.bfloat16), 'fs', axis=0, tiled=True)]
  transfers between devices with their start and end apart: 3 -> 0, of which waited for: 2 -> 0; matrix products, arithmetic and copies ran while one was open for 1% -> 0% of each run, Pallas kernels for 0% -> 0%
where the time goes in v1:
time: 245 us
  Pallas kernels  234 us (96%)
  other arithmetic  7.41 us (3%)
  local copies, waits for them, and re-layouts  3.52 us (1%)
    pallas_call x1, Pallas kernels, fused(): pl.pallas_call(functools.partial(kernel, nz), out_shape=jax.ShapeDtypeStr...  234 us

profile of v1, /device:TPU:0, one launch (start us, length us, event | category | flops | bytes accessed | tf_op | source)
XLA Modules:
  0.0 245.1 jit_solution(6468234103541533956)
XLA Ops:
  0.0 0.0 copy-start.4
  0.0 0.0 copy-start.1
  0.0 0.0 copy-start.2
  0.0 0.0 copy-start.5
  0.0 2.7 %fusion = f32[768]{0:T(1024)S(1)} fusion(bf16[768,2048]{1,0:T(8,128)(2,1)} %param.6), kind=kLoop, calls=%fused_computation.2 | loop fusion | flops 4717824 | bytes 3148800 | tf_op jit(solution)/shard_map/reduce_sum | solution.py:15
  2.7 0.0 copy-done.4
  2.8 0.6 dynamic_slice.3
  3.4 0.0 copy-done.1
  3.4 0.0 copy-start
  3.4 0.0 copy-start.3
  3.4 1.1 convert_element_type.14.up_ref
  4.5 0.0 copy-done.2
  4.5 0.0 copy-done.5
  4.5 1.1 multiply_convert_fusion.down_ref
  5.6 0.2 copy-done
  5.8 0.0 copy-done.3
  5.8 2.4 fusion.2.x_ref
  8.3 234.2 %shard_map.64 = bf16[768,1024]{1,0:T(8,128)(2,1)} custom-call(bf16[768,2048]{1,0:T(8,128)(2,1)} %fusion.2.x_ref, f32[1,2048]{1,0:T(1,128)} %bitcast.1, bf16[128,4096]{1,0:T(8,128)(2,1)} %convert_element_type.14.up_ref, bf16[4096,128]{1,0:T(8,128)(2,1)} %multiply_convert_fusion.down_ref), custom_call_target="tpu_custom_call" | custom-call | tf_op jit(solution)/shard_map/pallas_call | solution.py:281
  242.5 2.7 %copy.8 = bf16[768,1024]{1,0:T(8,128)(2,1)} copy(bf16[768,1024]{1,0:T(8,128)(2,1)} %shard_map.64) | data formatting | bytes 3145728
  (1 shorter events, 0.0 us)
Async XLA Ops:
  0.0 2.7 %copy-start.4 = (f32[4096]{0:T(1024)S(1)}, f32[4096]{0:T(1024)}, u32[]{:S(2)}) copy-start(f32[4096]{0:T(1024)} %param.9) | copy-start | bytes 49156
  0.0 3.4 %copy-start.1 = (f32[128,4096]{1,0:T(8,128)S(1)}, f32[128,4096]{1,0:T(8,128)}, u32[]{:S(2)}) copy-start(f32[128,4096]{1,0:T(8,128)} %param.8) | copy-start | bytes 6291460
  0.0 4.5 %copy-start.2 = (f32[4096,128]{1,0:T(8,128)S(1)}, f32[4096,128]{1,0:T(8,128)}, u32[]{:S(2)}) copy-start(f32[4096,128]{1,0:T(8,128)} %param.10) | copy-start | bytes 6291460
  0.0 4.5 %copy-start.5 = (f32[128]{0:T(128)S(1)}, f32[128]{0:T(128)}, u32[]{:S(2)}) copy-start(f32[128]{0:T(128)} %param.11) | copy-start | bytes 1540
  3.4 2.5 %copy-start = (bf16[768,2048]{1,0:T(8,128)(2,1)S(1)}, bf16[768,2048]{1,0:T(8,128)(2,1)}, u32[]{:S(2)}) copy-start(bf16[768,2048]{1,0:T(8,128)(2,1)} %param.6) | copy-start | bytes 9437188
  3.4 2.5 %copy-start.3 = (f32[2048]{0:T(1024)S(1)}, f32[2048]{0:T(1024)}, u32[]{:S(2)}) copy-start(f32[2048]{0:T(1024)} %param.7) | copy-start | bytes 24580

commit v2 on v1

--- a/solution.py
+++ b/solution.py
@@ -42,7 +42,7 @@
     z = me // (NX * NY)
     rows = x_ref.shape[0]
     depth = up_ref.shape[0]
-    wide = up_ref.shape[1] // NX
+    wide = up_ref.shape[1] // 2
     cols = down_ref.shape[1]
     pair = NX * cols
 
@@ -53,20 +53,24 @@
         return lax.rem(v + 2 * nz, nz)
 
     target = {
-        "z+": {"fs": fs_of(wrap(z + 1), y, x), "tp": c},
-        "z-": {"fs": fs_of(wrap(z - 1), y, x), "tp": c},
+        **{k: {"fs": fs_of(wrap(z + k), y, x), "tp": c} for k in range(1, nz)},
         "y": {"fs": fs_of(z, 1 - y, x), "tp": c},
         "x": {"fs": fs_of(z, y, 1 - x), "tp": c},
         "c": {"fs": me, "tp": 1 - c},
     }
 
+    side = lax.rem(z, 2)
+    peer = {"fs": fs_of(z + 1 - 2 * side, y, x), "tp": c}
+
+    def half_of(k):
+        at = pl.multiple_of(lax.rem(z + k, 2) * wide, wide)
+        return up_ref.at[:, pl.ds(at, wide)], down_ref.at[pl.ds(at, wide), :]
+
+    own_up = u_buf.at[pl.ds(pl.multiple_of(me * depth, depth), depth), :]
+    own_down = d_buf.at[me // NX, :, pl.ds(pl.multiple_of(x * cols, cols), cols)]
     local = [
-        pltpu.make_async_copy(
-            up_ref.at[:, pl.ds(pl.multiple_of(x * wide, wide), wide)],
-            u_buf.at[pl.ds(pl.multiple_of(me * depth, depth), depth), :], local_sems.at[0]),
-        pltpu.make_async_copy(
-            down_ref.at[pl.ds(pl.multiple_of(x * wide, wide), wide), :],
-            d_buf.at[me // NX, :, pl.ds(pl.multiple_of(x * cols, cols), cols)], local_sems.at[1]),
+        pltpu.make_async_copy(half_of(0)[0], own_up, local_sems.at[0]),
+        pltpu.make_async_copy(half_of(0)[1], own_down, local_sems.at[1]),
     ]
     for copy in local:
         copy.start()
@@ -82,7 +86,7 @@
         n = slots.setdefault(key, len(slots))
         return pltpu.make_async_remote_copy(
             src_ref=src, dst_ref=dst, send_sem=send_sems.at[n], recv_sem=recv_sems.at[n],
-            device_id=target[way], device_id_type=pl.DeviceIdType.MESH)
+            device_id=peer if way == "peer" else target[way], device_id_type=pl.DeviceIdType.MESH)
 
     def launch(key, src, dst, way):
         copy = copy_of(key, src, dst, way)
@@ -92,9 +96,9 @@
     def arrive(key, dst, way="x"):
         copy_of(key, dst, dst, way).wait_recv()
 
-    def block(kind, part, dz, dy, half):
-        zz, yy = wrap(z + dz), lax.rem(y + dy, NY)
-        xx = x if part == "A" else 1 - x
+    def block(kind, dz, px, py, half=None):
+        zz, yy = wrap(z + dz), lax.rem(y + py, NY)
+        xx = lax.rem(x + px, NX)
         if kind == "U":
             size = depth if half is None else depth // 2
             at = fs_of(zz, yy, xx) * depth + (0 if half in (None, 0) else size)
@@ -103,80 +107,53 @@
         at = 0 if half in (None, 0) else size
         return d_buf.at[zz * NY + yy, pl.ds(at, size), pl.ds(pl.multiple_of(xx * cols, cols), cols)]
 
-    def send(kind, part, dz, dy, way, half=None):
-        ref = block(kind, part, dz, dy, half)
-        to = {"z+": ((dz - 1) % nz, dy), "z-": ((dz + 1) % nz, dy), "y": (dz % nz, 1 - dy)}[way]
-        launch((kind, part) + to + (half,), ref, ref, way)
-
-    def take(kind, part, dz, dy, half=None):
-        arrive((kind, part, dz % nz, dy, half), block(kind, part, dz, dy, half))
-
-    def g1(k):
-        for way in ("z+", "z-", "y"):
-            send(k, "A", 0, 0, way)
-
-    def g2(k):
-        take(k, "B", 0, 0)
-        for way in ("y", "z+", "z-"):
-            send(k, "B", 0, 0, way)
-
-    def g3(k):
-        for dz, way, half in ((-1, "z+", 0), (1, "z-", 1)):
-            take(k, "A", dz, 0)
-            send(k, "A", dz, 0, way, half)
-            send(k, "A", dz, 0, "y")
-
-    def g4(k):
-        take(k, "B", 0, 1)
-        for way in ("z+", "z-"):
-            send(k, "B", 0, 1, way)
-
-    def g5(k):
-        for dz, way, half in ((-1, "z+", 0), (1, "z-", 1)):
-            take(k, "B", dz, 0)
-            send(k, "B", dz, 0, way, half)
-
-    def g6(k):
-        take(k, "A", 2, 0, 0)
-        take(k, "A", 2, 0, 1)
-        send(k, "A", 2, 0, "y")
-
-    def g7(k):
-        for dz, way, half in ((-1, "z+", 0), (1, "z-", 1)):
-            take(k, "B", dz, 1)
-            send(k, "B", dz, 1, way, half)
-
-    launch(("U", "B", 0, 0, None),
-           up_ref.at[:, pl.ds(pl.multiple_of((1 - x) * wide, wide), wide)],
-           u_buf.at[pl.ds(pl.multiple_of(me * depth, depth), depth), :], "x")
+    def column(kind, *ways):
+        for k in ways:
+            src, dst = (half_of(k)[0], own_up) if kind == "U" else (half_of(k)[1], own_down)
+            launch((kind, nz - k, 0, 0, None), src, dst, k)
+
+    def take(kind, dz, px, py, half=None):
+        arrive((kind, dz, px, py, half), block(kind, dz, px, py, half))
+
+    def share(kind, dz):
+        if dz:
+            take(kind, dz, 0, 0)
+        ref = block(kind, dz, 0, 0)
+        launch((kind, dz, 1, 0, None), ref, ref, "x")
+        launch((kind, dz, 0, 1, None), ref, ref, "y")
+
+    def cross(kind, dz):
+        for px, py, way, half in ((1, 0, "y", 0), (0, 1, "x", 1)):
+            take(kind, dz, px, py)
+            ref = block(kind, dz, px, py, half)
+            launch((kind, dz, 1, 1, half), ref, ref, way)
+
+    def corner(kind, dz):
+        take(kind, dz, 1, 1, 0)
+        take(kind, dz, 1, 1, 1)
+
     part_rows = rows // 2
     mine_rows = pl.ds(pl.multiple_of(c * part_rows, part_rows), part_rows)
     other_rows = pl.ds(pl.multiple_of((1 - c) * part_rows, part_rows), part_rows)
-    launch(("T", "x"), x_ref.at[mine_rows, :], t_buf.at[mine_rows, :], "x")
-    launch(("D", "B", 0, 0, None),
-           down_ref.at[pl.ds(pl.multiple_of((1 - x) * wide, wide), wide), :],
-           d_buf.at[me // NX, :, pl.ds(pl.multiple_of(x * cols, cols), cols)], "x")
-
+    column("U", 1, 3)
     local[0].wait()
-    g1("U")
-    g2("U")
-    g3("U")
-    g4("U")
-    g5("U")
-    g6("U")
-    g7("U")
+    share("U", 0)
+    cross("U", 0)
+    share("U", 1)
+    share("U", 3)
+    column("U", 2)
+    launch(("T", "x"), x_ref.at[mine_rows, :], t_buf.at[mine_rows, :], "peer")
+    cross("U", 1)
+    share("U", 2)
+    column("D", 1, 3)
+    cross("U", 3)
     local[1].wait()
-    g1("D")
+    share("D", 0)
+    cross("U", 2)
     arrive(("T", "x"), t_buf.at[mine_rows, :])
     launch(("T", "c"), t_buf.at[mine_rows, :], t_buf.at[mine_rows, :], "c")
-    take("U", "A", 0, 1)
-    take("U", "A", -1, 1)
-    take("U", "A", 1, 1)
-    for half in (0, 1):
-        take("U", "B", 2, 0, half)
-        take("U", "B", 2, 1, half)
-    take("U", "A", 2, 1)
-    arrive(("T", "c"), t_buf.at[other_rows, :])
+    for dz in range(nz):
+        corner("U", dz)
 
     tile_m, tile_n = 256, min(512, wide)
 
@@ -194,13 +171,15 @@
                 h_buf[pl.ds(base + r, tile_m), at] = act.astype(jnp.bfloat16)
 
     up_part(x_ref, 0)
-    g2("D")
-    g3("D")
+    cross("D", 0)
+    share("D", 1)
+    share("D", 3)
+    column("D", 2)
+    arrive(("T", "c"), t_buf.at[other_rows, :])
     up_part(t_buf, rows)
-    g4("D")
-    g5("D")
-    g6("D")
-    g7("D")
+    cross("D", 1)
+    share("D", 2)
+    cross("D", 3)
 
     stages = [((z + 1) % 2, 0), ((z + 1) % 2, 1), (z % 2, 0), (z % 2, 1)]
 
@@ -211,7 +190,7 @@
     def theirs(n):
         zy = owned(n, 1 - c)
 
-        @pl.loop(0, NX * rows // tile_m)
+        @pl.loop(0, 2 * rows // tile_m)
         def _(i):
             r = pl.ds(pl.multiple_of(i * tile_m, tile_m), tile_m)
             ssend[n, r, :] = jnp.dot(h_buf[r, :], d_buf[zy],
@@ -233,7 +212,8 @@
             r = pl.multiple_of(i * tile_m, tile_m)
             xsend[n, pl.ds(r, tile_m), :] = total(rows + r).astype(jnp.bfloat16)
 
-        launch(("X", n), xsend.at[n], xrecv.at[n], "x")
+        met = (n + 2) % 4
+        launch(("X", met), xsend.at[n], xrecv.at[met], "peer")
 
         @pl.loop(0, rows // tile_m)
         def _(i):
@@ -246,25 +226,20 @@
         out_ref[:, pl.ds(at, pair)] = (keep[n] + xrecv[n].astype(jnp.float32)).astype(out_ref.dtype)
 
     theirs(0)
-    take("D", "A", 0, 1)
-    take("D", "A", -1, 1)
-    take("D", "A", 1, 1)
+    corner("D", 1)
+    corner("D", 3)
     theirs(1)
     mine(0)
-    take("D", "B", 2, 0, 0)
-    take("D", "B", 2, 0, 1)
+    cross("D", 2)
     theirs(2)
     mine(1)
-    finish(0)
-    take("D", "A", 2, 1)
-    take("D", "B", 2, 1, 0)
-    take("D", "B", 2, 1, 1)
+    corner("D", 0)
+    corner("D", 2)
     theirs(3)
     mine(2)
     mine(3)
-    finish(1)
-    finish(2)
-    finish(3)
+    for n in (2, 3, 0, 1):
+        finish(n)
     for copy in started:
         copy.wait_send()
 
@@ -273,10 +248,10 @@
     rows, width = tokens.shape
     depth, hidden = up_weight.shape
     cols = down_weight.shape[1]
-    wide = hidden // NX
-    x = lax.rem(lax.axis_index("fs"), NX)
-    own_scale = lax.dynamic_slice_in_dim(up_scale, x * wide, wide, 0)[None]
-    ways = 2 * (8 + 10) + 2 + 8
+    wide = hidden // 2
+    side = lax.rem(lax.axis_index("fs") // (NX * NY), 2)
+    own_scale = lax.dynamic_slice_in_dim(up_scale, side * wide, wide, 0)[None]
+    ways = 2 * (nz - 1 + 4 * nz) + 2 + 8
     vmem = pl.BlockSpec(memory_space=pltpu.VMEM)
     return pl.pallas_call(
         functools.partial(kernel, nz),
@@ -287,9 +262,9 @@
             pltpu.VMEM((width, wide), jnp.bfloat16),
             pltpu.VMEM((nz * NY, wide, NX * cols), jnp.bfloat16),
             pltpu.VMEM((rows, width), jnp.bfloat16),
-            pltpu.VMEM((NX * rows, wide), jnp.bfloat16),
-            pltpu.VMEM((4, NX * rows, NX * cols), jnp.bfloat16),
-            pltpu.VMEM((4, NX * rows, NX * cols), jnp.bfloat16),
+            pltpu.VMEM((2 * rows, wide), jnp.bfloat16),
+            pltpu.VMEM((4, 2 * rows, NX * cols), jnp.bfloat16),
+            pltpu.VMEM((4, 2 * rows, NX * cols), jnp.bfloat16),
             pltpu.VMEM((4, rows, NX * cols), jnp.bfloat16),
             pltpu.VMEM((4, rows, NX * cols), jnp.bfloat16),
             pltpu.VMEM((4, rows, NX * cols), jnp.float32),

time: 245 us -> 206 us (0.84)
  Pallas kernels: 234 us -> 195 us
    pallas_call x1, Pallas kernels: 234 us -> 195 us  [fused(): pl.pallas_call(functools.partial(kernel, nz), out_shape=jax.ShapeDtypeStr...]
where the time goes in v2:
time: 206 us
  Pallas kernels  195 us (95%)
  other arithmetic  7.41 us (4%)
  local copies, waits for them, and re-layouts  3.52 us (2%)
    pallas_call x1, Pallas kernels, fused(): pl.pallas_call(functools.partial(kernel, nz), out_shape=jax.ShapeDtypeStr...  195 us

profile of v2, /device:TPU:0, one launch (start us, length us, event | category | flops | bytes accessed | tf_op | source)
XLA Modules:
  0.0 206.2 jit_solution(1550454538272228547)
XLA Ops:
  0.0 0.0 copy-start.4
  0.0 0.0 copy-start.1
  0.0 0.0 copy-start.2
  0.0 0.0 copy-start.5
  0.0 2.7 %fusion = f32[768]{0:T(1024)S(1)} fusion(bf16[768,2048]{1,0:T(8,128)(2,1)} %param.6), kind=kLoop, calls=%fused_computation.2 | loop fusion | flops 4717824 | bytes 3148800 | tf_op jit(solution)/shard_map/reduce_sum | solution.py:15
  2.7 0.0 copy-done.4
  2.8 0.6 dynamic_slice.3
  3.4 0.0 copy-done.1
  3.4 0.0 copy-start
  3.4 0.0 copy-start.3
  3.4 1.1 convert_element_type.14.up_ref
  4.5 0.0 copy-done.2
  4.5 0.0 copy-done.5
  4.5 1.1 multiply_convert_fusion.down_ref
  5.6 0.2 copy-done
  5.8 0.0 copy-done.3
  5.8 2.4 %fusion.2.x_ref = bf16[768,2048]{1,0:T(8,128)(2,1)} fusion(bf16[768,2048]{1,0:T(8,128)(2,1)S(1)} %copy-done, f32[2048]{0:T(1024)S(1)} %copy-done.3, f32[768]{0:T(1024)S(1)} %add_rsqrt_fusion), kind=kLoop, calls=%fused_computation.4 | loop fusion | flops 6291456 | bytes 6302720 | tf_op jit(solution)/shard_map/convert_element_type | solution.py:16
  8.3 195.2 %shard_map.64 = bf16[768,1024]{1,0:T(8,128)(2,1)} custom-call(bf16[768,2048]{1,0:T(8,128)(2,1)} %fusion.2.x_ref, f32[1,2048]{1,0:T(1,128)} %bitcast.1, bf16[128,4096]{1,0:T(8,128)(2,1)} %convert_element_type.14.up_ref, bf16[4096,128]{1,0:T(8,128)(2,1)} %multiply_convert_fusion.down_ref), custom_call_target="tpu_custom_call" | custom-call | tf_op jit(solution)/shard_map/pallas_call | solution.py:256
  203.5 2.7 %copy.8 = bf16[768,1024]{1,0:T(8,128)(2,1)} copy(bf16[768,1024]{1,0:T(8,128)(2,1)} %shard_map.64) | data formatting | bytes 3145728
  (1 shorter events, 0.0 us)
Async XLA Ops:
  0.0 2.7 %copy-start.4 = (f32[4096]{0:T(1024)S(1)}, f32[4096]{0:T(1024)}, u32[]{:S(2)}) copy-start(f32[4096]{0:T(1024)} %param.9) | copy-start | bytes 49156
  0.0 3.4 %copy-start.1 = (f32[128,4096]{1,0:T(8,128)S(1)}, f32[128,4096]{1,0:T(8,128)}, u32[]{:S(2)}) copy-start(f32[128,4096]{1,0:T(8,128)} %param.8) | copy-start | bytes 6291460
  0.0 4.5 %copy-start.2 = (f32[4096,128]{1,0:T(8,128)S(1)}, f32[4096,128]{1,0:T(8,128)}, u32[]{:S(2)}) copy-start(f32[4096,128]{1,0:T(8,128)} %param.10) | copy-start | bytes 6291460
  0.0 4.5 %copy-start.5 = (f32[128]{0:T(128)S(1)}, f32[128]{0:T(128)}, u32[]{:S(2)}) copy-start(f32[128]{0:T(128)} %param.11) | copy-start | bytes 1540
  3.4 2.5 %copy-start = (bf16[768,2048]{1,0:T(8,128)(2,1)S(1)}, bf16[768,2048]{1,0:T(8,128)(2,1)}, u32[]{:S(2)}) copy-start(bf16[768,2048]{1,0:T(8,128)(2,1)} %param.6) | copy-start | bytes 9437188
  3.4 2.5 %copy-start.3 = (f32[2048]{0:T(1024)S(1)}, f32[2048]{0:T(1024)}, u32[]{:S(2)}) copy-start(f32[2048]{0:T(1024)} %param.7) | copy-start | bytes 24580
